TPU v7x, 32 devices: a whole 2x2x4 slice. The times are simulated.
32 devices in a mesh: ep: 8 (over z, y), tp: 4 (over x, core).
Axes of the slice: x: 2, y: 2, z: 4, core: 2. Of those that a mesh axis runs over, the one named last changes fastest.
Arguments:
- outer_gate: bfloat16 [4096, 2048], P('ep', 'tp'), may hold values from -6 to 6
- inner_gate: bfloat16 [4096, 2048], P('ep', 'tp'), may hold values from -6 to 6
- conv_values: bfloat16 [4096, 2048], P('ep', 'tp'), may hold values from -6 to 6
- conv_taps: bfloat16 [3, 2048], P(None, 'tp'), may hold values from -3 to 3
- out_weight: bfloat16 [2048, 2048], P('tp'), may hold values from -0.125 to 0.125
- moe_input: bfloat16 [4096, 2048], P(('ep', 'tp')), may hold values from -6 to 6
- norm_gain: bfloat16 [2048], replicated, may hold values from 0.099609375 to 1.8984375
- gate_proj: bfloat16 [8, 2048, 1024], P('ep', None, 'tp'), may hold values from -0.125 to 0.125
- up_proj: bfloat16 [8, 2048, 1024], P('ep', None, 'tp'), may hold values from -0.125 to 0.125
- down_proj: bfloat16 [8, 1024, 2048], P('ep', 'tp'), may hold values from -0.1875 to 0.1875
- shared_gate: bfloat16 [2048, 1024], P(None, 'tp'), may hold values from -0.125 to 0.125
- shared_up: bfloat16 [2048, 1024], P(None, 'tp'), may hold values from -0.125 to 0.125
- shared_down: bfloat16 [1024, 2048], P('tp'), may hold values from -0.1875 to 0.1875
- routes: int32 [4096, 2], P('ep'), may hold values from 0 to 7, all different within a row; in each aligned block of 128 rows (0 to 127, 128 to 255, ...) at most 64 rows name the same one
- route_weight: float32 [4096, 2], P('ep'), may hold values from 0.3 to 1.5
Outputs:
- mixer_out: bfloat16 [4096, 2048], P(('ep', 'tp'))
- expert_mix: bfloat16 [4096, 2048], P(('ep', 'tp'))
Inputs may be any that keep to these rules, and one draw needn't show every extreme that they name: `routes`: each row names 2 different experts. In the 128 rows of one device no expert is named more than 64 times, and in every draw some expert is named exactly 64 times in one device's rows.
All inputs are finite; a program needn't handle non-finite values.
Results may differ from a plain program's by a relative error of at most 0.012.
Values may be sent and summed in bfloat16 or wider, within the bound.
A program may use at most 128 MiB of HBM per device.

v0:
```python
from functools import partial

import jax
import jax.numpy as jnp
from jax import lax
from jax.sharding import PartitionSpec as P

epsilon = 1e-06


def shifted(block, axis, distance):
    devices = range(lax.axis_size(axis))
    route = [(i - distance, i) for i in devices if i - distance in devices]
    return lax.ppermute(block, axis, route)


def rms_norm(inputs, scales):
    values = inputs.astype(jnp.float32)
    square = jnp.mean(values * values, axis=-1, keepdims=True)
    return (values * lax.rsqrt(square + epsilon) * scales.astype(jnp.float32)).astype(jnp.bfloat16)


def swiglu(inputs, gate_w, up_w):
    gate_term = jnp.dot(inputs, gate_w, preferred_element_type=jnp.float32)
    upward = jnp.dot(inputs, up_w, preferred_element_type=jnp.float32)
    return (jax.nn.silu(gate_term) * upward).astype(jnp.bfloat16)


def slot_table(block_routes, experts, capacity):
    flat_ids = block_routes.reshape(-1)
    onehot = (flat_ids[:, None] == jnp.arange(experts, dtype=jnp.int32)[None, :]).astype(jnp.int32)
    earlier = jnp.cumsum(onehot, axis=0) - onehot
    slot_ids = jnp.sum(earlier * onehot, axis=1)
    targets = flat_ids * capacity + slot_ids
    owners = jnp.arange(flat_ids.shape[0], dtype=jnp.int32) // block_routes.shape[1]
    sources = jnp.zeros((experts * capacity,), jnp.int32).at[targets].set(owners)
    filled = jnp.zeros((experts * capacity,), jnp.bfloat16).at[targets].set(1.0)
    return (sources, filled, targets)


def send_own(normed, own_routes, table_maker, ep_count, capacity):
    sources, filled, own_targets = table_maker(own_routes)
    outgoing = (normed[sources] * filled[:, None]).reshape(ep_count, capacity, normed.shape[1])
    landed = lax.all_to_all(outgoing, "ep", split_axis=0, concat_axis=0, tiled=True)
    return (landed, own_targets)


def per_device(
    outer_gate,
    inner_gate,
    conv_values,
    conv_taps,
    out_weight,
    moe_input,
    norm_gain,
    gate_proj,
    up_proj,
    down_proj,
    shared_gate,
    shared_up,
    shared_down,
    routes,
    route_weight,
):
    tp_count = lax.axis_size("tp")
    ep_count = lax.axis_size("ep")
    my_slot = lax.axis_index("tp")
    group_len = inner_gate.shape[0]
    mix_rows = group_len // tp_count
    channels = inner_gate.shape[1]
    model_width = moe_input.shape[1]
    own_rows = moe_input.shape[0]
    top_count = routes.shape[1]
    capacity = 2 * own_rows * top_count // ep_count
    slot_rows = ep_count * capacity
    reach_rows = conv_taps.shape[0] - 1
    edge_rows = jnp.stack(
        (inner_gate[group_len - reach_rows :], conv_values[group_len - reach_rows :])
    )
    before = shifted(edge_rows, "ep", 1)
    full_gate = jnp.concatenate((before[0], inner_gate), axis=0).astype(jnp.float32)
    full_values = jnp.concatenate((before[1], conv_values), axis=0).astype(jnp.float32)
    product = full_gate * full_values
    tap_values = conv_taps.astype(jnp.float32)
    convolved = tap_values[0] * product[0:group_len]
    for offset in range(1, reach_rows + 1):
        convolved = convolved + tap_values[offset] * product[offset : offset + group_len]
    gate_rows = (outer_gate.astype(jnp.float32) * convolved).astype(jnp.bfloat16)
    gate_rows = gate_rows.reshape(tp_count, mix_rows, channels)
    normed = rms_norm(moe_input, norm_gain)
    group_normed = lax.all_gather(normed, "tp", axis=0, tiled=True)
    group_split = group_normed.reshape(tp_count, own_rows, model_width)
    own_weights = lax.dynamic_slice_in_dim(route_weight, my_slot * own_rows, own_rows, 0)
    own_routes = lax.dynamic_slice_in_dim(routes, my_slot * own_rows, own_rows, 0)
    table_maker = partial(slot_table, experts=ep_count, capacity=capacity)
    local_routed = None
    landed, own_targets = send_own(normed, own_routes, table_maker, ep_count, capacity)
    gate_full, up_full, down_full = (
        lax.all_gather(gate_proj, "tp", axis=2, tiled=True),
        lax.all_gather(up_proj, "tp", axis=2, tiled=True),
        lax.all_gather(down_proj, "tp", axis=1, tiled=True),
    )
    hidden = swiglu(landed.reshape(slot_rows, model_width), gate_full[0], up_full[0])
    unit_block = hidden.shape[1] // tp_count
    local_routed = jnp.zeros((slot_rows, model_width), jnp.float32)
    for piece_idx in range(tp_count):
        partial_sum = jnp.dot(
            hidden[:, piece_idx * unit_block : (piece_idx + 1) * unit_block],
            down_full[0, piece_idx * unit_block : (piece_idx + 1) * unit_block],
            preferred_element_type=jnp.float32,
        ).astype(jnp.bfloat16)
        local_routed = local_routed + partial_sum.astype(jnp.float32)
    routed_rows = 0
    expert_block = routed_rows + own_rows
    joint_block = mix_rows + expert_block
    dev_count = joint_block * lax.axis_size("tp") // joint_block
    block_rows = gate_rows
    block_rows = block_rows.reshape(dev_count * mix_rows, channels)
    projected = jnp.dot(block_rows, out_weight, preferred_element_type=jnp.float32)
    shared_in = group_split
    shared_in = shared_in.reshape(dev_count * own_rows, model_width)
    shared_out = jnp.dot(
        swiglu(shared_in, shared_gate, shared_up), shared_down, preferred_element_type=jnp.float32
    )
    shared_out = shared_out.reshape(dev_count, own_rows, model_width)
    combined = jnp.concatenate(
        (projected.reshape(dev_count, mix_rows, model_width), shared_out), axis=1
    )
    summed = lax.psum_scatter(
        combined.reshape(dev_count * joint_block, model_width).astype(jnp.bfloat16),
        "tp",
        scatter_dimension=0,
        tiled=True,
    ).astype(jnp.float32)
    mixer_out = summed[:mix_rows].astype(jnp.bfloat16)
    expert_total = summed[mix_rows:]
    routed_back = local_routed.astype(jnp.bfloat16)
    routed_back = routed_back.reshape(ep_count, capacity, model_width)
    returned = lax.all_to_all(routed_back, "ep", split_axis=0, concat_axis=0, tiled=True).reshape(
        slot_rows, model_width
    )
    picked = returned[own_targets].reshape(own_rows, top_count, model_width).astype(jnp.float32)
    routed = jnp.sum(picked * own_weights[:, :, None], axis=1)
    expert_mix = (expert_total + routed).astype(jnp.bfloat16)
    return (mixer_out, expert_mix)


def solution(mesh):
    return jax.shard_map(
        per_device,
        mesh=mesh,
        in_specs=(
            P("ep", "tp"),
            P("ep", "tp"),
            P("ep", "tp"),
            P(None, "tp"),
            P("tp", None),
            P(("ep", "tp"), None),
            P(),
            P("ep", None, "tp"),
            P("ep", None, "tp"),
            P("ep", "tp", None),
            P(None, "tp"),
            P(None, "tp"),
            P("tp", None),
            P("ep", None),
            P("ep", None),
        ),
        out_specs=(P(("ep", "tp"), None), P(("ep", "tp"), None)),
        check_vma=False,
    )
```

profile of v0, /device:TPU:0, one launch (start us, length us, event | category | flops | bytes accessed | tf_op | source)
XLA Modules:
  0.0 229.2 jit_solution(8211461132235295244)
XLA Ops:
  7.2 0.8 convert_element_type.85
  8.1 1.2 fusion.7
  9.3 2.0 fusion.9
  11.4 0.7 all-gather.7.cloned.1.call-update
  13.4 0.7 broadcast_multiply_fusion.1
  15.7 1.4 scatter_custom_fusion
  17.2 3.3 %gather_fusion = bf16[512,2048]{1,0:T(8,128)(2,1)} fusion(bf16[128,2048]{1,0:T(8,128)(2,1)S(1)} %copy-done.1, s32[1024]{0:T(1024)S(1)} %pad_clamp_fusion.1), kind=kCustom, calls=%fused_computation | custom fusion | bytes 4196352 | tf_op jit(solution)/shard_map/gather | solution.py:43
  20.5 2.2 scatter_custom_fusion.1
  22.7 3.1 %broadcast_multiply_fusion = bf16[8,64,2048]{2,1,0:T(8,128)(2,1)} fusion(bf16[8,64,2048]{2,1,0:T(8,128)(2,1)} %bitcast.58, bf16[8,64]{1,0:T(8,128)(2,1)S(1)} %mul.134), kind=kLoop, calls=%fused_computation.38 | loop fusion | flops 1048576 | bytes 4195328 | tf_op jit(solution)/shard_map/mul | solution.py:43
  25.8 7.4 %all-to-all-start = ((bf16[8,64,2048]{2,1,0:T(8,128)(2,1)}), bf16[8,64,2048]{2,1,0:T(8,128)(2,1)}, u32[]{:S(2)}, u32[]{:S(2)}) async-start(bf16[8,64,2048]{2,1,0:T(8,128)(2,1)} %broadcast_multiply_fusion), calls=%async_computation.1 | async-start | bytes 4194304 | tf_op jit(solution)/shard_map/all_to_all | solution.py:44
  33.4 4.2 %collective-permute-start = (bf16[2,2,512]{2,1,0:T(2,128)(2,1)S(1)}, bf16[2,2,512]{2,1,0:T(2,128)(2,1)S(1)}, u32[]{:S(2)}, u32[]{:S(2)}) collective-permute-start(bf16[2,2,512]{2,1,0:T(2,128)(2,1)S(1)} %pad_maximum_fusion.1), channel_id=1, source_target_pairs={{0,4},{4,8},{8,12},{12,16},{16,20},{20,24},{24,28},{1,5},{5,9},{9,... | collective-permute-start | bytes 12296 | tf_op jit(solution)/shard_map/ppermute | solution.py:14
  37.6 12.8 %collective-permute-done = bf16[2,2,512]{2,1,0:T(2,128)(2,1)S(1)} collective-permute-done((bf16[2,2,512]{2,1,0:T(2,128)(2,1)S(1)}, bf16[2,2,512]{2,1,0:T(2,128)(2,1)S(1)}, u32[]{:S(2)}, u32[]{:S(2)}) %collective-permute-start) | collective-permute-done | bytes 4128 | tf_op jit(solution)/shard_map/ppermute | solution.py:14
  50.7 2.8 %convolution_convert_fusion.5 = bf16[512,2048]{1,0:T(8,128)(2,1)} fusion(bf16[512,2048]{1,0:T(8,128)(2,1)S(1)} %copy-done, f32[514,512]{1,0:T(8,128)S(1)} %convert_multiply_fusion.2, bf16[512,512]{1,0:T(8,128)(2,1)S(1)} %copy-done.7, f32[512]{0:T(512)S(1)} %bitcast.67, f32[512]{0:T(512)S(1)} %bitcast.66, f32[512]{0:T(512)S(1)} %bitcast.65), kind=kOutput, calls=%fused_computation.15 | convolution fusion | flops 1076887552 | bytes 7870464 | tf_op jit(solution)/shard_map/dot_general | solution.py:119
  53.5 3.1 %fusion.37 = f32[512,256]{1,0:T(8,128)} fusion(bf16[512,2048]{1,0:T(8,128)(2,1)} %all-gather.5.cloned.1.call-done, bf16[2048,256]{1,0:T(8,128)(2,1)S(1)} %copy-done.6), kind=kOutput, calls=%fused_computation.82 | convolution fusion | flops 536870912 | bytes 3670016 | tf_op jit(solution)/shard_map/dot_general | solution.py:24
  56.6 6.0 %convolution_convert_fusion.4 = bf16[512,2048]{1,0:T(8,128)(2,1)} fusion(bf16[256,2048]{1,0:T(8,128)(2,1)} %param.27, bf16[512,2048]{1,0:T(8,128)(2,1)} %all-gather.5.cloned.1.call-done, bf16[2048,256]{1,0:T(8,128)(2,1)} %param.26, f32[512,256]{1,0:T(8,128)} %fusion.37), kind=kOutput, calls=%fused_computation.14 | convolution fusion | flops 1075576832 | bytes 6815744 | tf_op jit(solution)/shard_map/dot_general | solution.py:122
  62.6 4.8 %pad_maximum_fusion = bf16[4,256,2048]{2,1,0:T(8,128)(2,1)} fusion(bf16[4,128,2048]{2,1,0:T(8,128)(2,1)} %bitcast.60, bf16[4,128,2048]{2,1,0:T(8,128)(2,1)} %bitcast.59), kind=kLoop, calls=%fused_computation.4 | loop fusion | flops 8388608 | bytes 8388608 | tf_op jit(solution)/shard_map/concatenate | solution.py:126
  67.4 14.2 %all-to-all-done = bf16[8,64,2048]{2,1,0:T(8,128)(2,1)} async-done(((bf16[8,64,2048]{2,1,0:T(8,128)(2,1)}), bf16[8,64,2048]{2,1,0:T(8,128)(2,1)}, u32[]{:S(2)}, u32[]{:S(2)}) %all-to-all-start) | async-done | bytes 2097184 | tf_op jit(solution)/shard_map/all_to_all | solution.py:44
  81.6 7.2 %fusion.2 = f32[512,1024]{1,0:T(8,128)} fusion(bf16[512,2048]{1,0:T(8,128)(2,1)} %bitcast.15, bf16[1,2048,1024]{2,1,0:T(8,128)(2,1)} %all-gather.7.cloned.1.call-done), kind=kOutput, calls=%fused_computation.7 | convolution fusion | flops 2147483648 | bytes 8388608 | tf_op jit(solution)/shard_map/dot_general | solution.py:24
  88.8 21.2 %all-gather.9.cloned.1.call-done = bf16[1,2048,1024]{2,1,0:T(8,128)(2,1)} async-done(((bf16[1,2048,256]{2,1,0:T(8,128)(2,1)}), bf16[1,2048,1024]{2,1,0:T(8,128)(2,1)}) %all-gather.9.cloned.1.call-update) | async-done | bytes 4194320 | tf_op jit(solution)/shard_map/all_gather | solution.py:100
  110.0 5.9 %multiply_convert_fusion = bf16[512,1024]{1,0:T(8,128)(2,1)S(1)} fusion(f32[512,1024]{1,0:T(8,128)} %fusion.2, bf16[512,2048]{1,0:T(8,128)(2,1)} %bitcast.15, bf16[1,2048,1024]{2,1,0:T(8,128)(2,1)} %all-gather.9.cloned.1.call-done), kind=kOutput, calls=%fused_computation.17 | convolution fusion | flops 2150629376 | bytes 9437184 | tf_op jit(solution)/shard_map/dot_general | solution.py:25
  115.9 30.0 %all-gather.11.cloned.1.call-done = bf16[1,1024,2048]{2,1,0:T(8,128)(2,1)} async-done(((bf16[1,256,2048]{2,1,0:T(8,128)(2,1)}), bf16[1,1024,2048]{2,1,0:T(8,128)(2,1)}) %all-gather.11.cloned.1.call-update) | async-done | bytes 4194320 | tf_op jit(solution)/shard_map/all_gather | solution.py:101
  145.9 2.1 convolution_convert_fusion
  148.0 1.9 convolution_convert_fusion.1
  149.9 0.7 convolution_convert_fusion.2
  150.6 2.6 %add_convert_fusion = bf16[512,2048]{1,0:T(8,128)(2,1)} fusion(bf16[512,2048]{1,0:T(8,128)(2,1)S(1)} %convolution_convert_fusion, bf16[512,2048]{1,0:T(8,128)(2,1)S(1)} %convolution_convert_fusion.1, bf16[512,2048]{1,0:T(8,128)(2,1)S(1)} %convolution_convert_fusion.2, bf16[1,1024,2048]{2,1,0:T(8,128)(2,1)S(1)} %copy-done.2, ...), kind=kOutput, calls=%fused_computation.9 | convolution fusion | flops 546308096 | bytes 9699328 | tf_op jit(solution)/shard_map/dot_general | solution.py:107
  153.2 5.5 %all-to-all-start.1 = ((bf16[8,64,2048]{2,1,0:T(8,128)(2,1)}), bf16[8,64,2048]{2,1,0:T(8,128)(2,1)}, u32[]{:S(2)}, u32[]{:S(2)}) async-start(bf16[8,64,2048]{2,1,0:T(8,128)(2,1)} %bitcast.57), calls=%async_computation.2 | async-start | bytes 4194304 | tf_op jit(solution)/shard_map/all_to_all | solution.py:139
  159.5 47.9 %all-to-all-done.1 = bf16[8,64,2048]{2,1,0:T(8,128)(2,1)} async-done(((bf16[8,64,2048]{2,1,0:T(8,128)(2,1)}), bf16[8,64,2048]{2,1,0:T(8,128)(2,1)}, u32[]{:S(2)}, u32[]{:S(2)}) %all-to-all-start.1) | async-done | bytes 2097184 | tf_op jit(solution)/shard_map/all_to_all | solution.py:139
  207.5 4.2 %gather_fusion.1 = bf16[256,2048]{1,0:T(8,128)(2,1)S(1)} fusion(bf16[512,2048]{1,0:T(8,128)(2,1)} %bitcast.23, s32[1024]{0:T(1024)S(1)} %pad_clamp_fusion), kind=kCustom, calls=%fused_computation.1 | custom fusion | bytes 2098176 | tf_op jit(solution)/shard_map/gather | solution.py:142
  211.7 2.4 %reshape.96 = f32[128,2,2048]{2,1,0:T(2,128)} reshape(bf16[256,2048]{1,0:T(8,128)(2,1)S(1)} %gather_fusion.1) | data formatting | bytes 3145728 | tf_op jit(solution)/shard_map/convert_element_type | solution.py:142
  214.1 4.7 %multiply_reduce_fusion = f32[128,2048]{1,0:T(8,128)S(1)} fusion(f32[128,2,2048]{2,1,0:T(2,128)} %reshape.96, f32[128,2]{1,0:T(8,128)S(1)} %copy.21), kind=kLoop, calls=%fused_computation.16 | loop fusion | flops 786432 | bytes 3146752 | tf_op jit(solution)/shard_map/reduce_sum | solution.py:143
  218.8 1.9 slice.105
  220.7 1.9 add_convert_fusion.1
  (54 shorter events, 4.3 us)
Async XLA Ops:
  7.2 43.5 %copy-start = (bf16[512,2048]{1,0:T(8,128)(2,1)S(1)}, bf16[512,2048]{1,0:T(8,128)(2,1)}, u32[]{:S(2)}) copy-start(bf16[512,2048]{1,0:T(8,128)(2,1)} %param.19) | copy-start | bytes 6291460
  7.2 46.3 %all-gather.5.cloned.1.call-start = ((), (), s32[]{:S(2)}) async-start(), calls=%async_computation.3 | async-start | bytes 2621440 | tf_op jit(solution)/shard_map/all_gather | solution.py:91
  11.3 5.8 %copy-start.1 = (bf16[128,2048]{1,0:T(8,128)(2,1)S(1)}, bf16[128,2048]{1,0:T(8,128)(2,1)}, u32[]{:S(2)}) copy-start(bf16[128,2048]{1,0:T(8,128)(2,1)} %fusion.9) | copy-start | bytes 1572868
  11.3 70.3 %all-gather.7.cloned.1.call-start = ((), (), s32[]{:S(2)}) async-start(), calls=%async_computation.5 | async-start | bytes 5242880 | tf_op jit(solution)/shard_map/all_gather | solution.py:99
  12.1 97.9 %all-gather.9.cloned.1.call-start = ((), (), s32[]{:S(2)}) async-start(), calls=%async_computation.6 | async-start | bytes 5242880 | tf_op jit(solution)/shard_map/all_gather | solution.py:100
  12.8 133.0 %all-gather.11.cloned.1.call-start = ((), (), s32[]{:S(2)}) async-start(), calls=%async_computation.7 | async-start | bytes 5242880 | tf_op jit(solution)/shard_map/all_gather | solution.py:101
  25.8 7.5 %copy-start.3 = (bf16[512,512]{1,0:T(8,128)(2,1)S(1)}, bf16[512,512]{1,0:T(8,128)(2,1)}, u32[]{:S(2)}) copy-start(bf16[512,512]{1,0:T(8,128)(2,1)} %param.16) | copy-start | bytes 1572868
  25.8 7.5 %copy-start.4 = (bf16[512,512]{1,0:T(8,128)(2,1)S(1)}, bf16[512,512]{1,0:T(8,128)(2,1)}, u32[]{:S(2)}) copy-start(bf16[512,512]{1,0:T(8,128)(2,1)} %param.17) | copy-start | bytes 1572868
  25.8 11.8 %copy-start.5 = (bf16[3,512]{1,0:T(4,128)(2,1)S(1)}, bf16[3,512]{1,0:T(4,128)(2,1)}, u32[]{:S(2)}) copy-start(bf16[3,512]{1,0:T(4,128)(2,1)} %param.18) | copy-start | bytes 9220
  25.8 55.8 %all-to-all-start = ((bf16[8,64,2048]{2,1,0:T(8,128)(2,1)}), bf16[8,64,2048]{2,1,0:T(8,128)(2,1)}, u32[]{:S(2)}, u32[]{:S(2)}) async-start(bf16[8,64,2048]{2,1,0:T(8,128)(2,1)} %broadcast_multiply_fusion), calls=%async_computation.1 | async-start | bytes 4194304 | tf_op jit(solution)/shard_map/all_to_all | solution.py:44
  33.3 185.6 %reduce-scatter.2.cloned.1.call-start = ((), (), s32[]{:S(2)}) async-start(), calls=%async_computation.4 | async-start | bytes 5242880 | tf_op jit(solution)/shard_map/reduce_scatter | solution.py:129
  33.3 17.4 %copy-start.7 = (bf16[512,512]{1,0:T(8,128)(2,1)S(1)}, bf16[512,512]{1,0:T(8,128)(2,1)}, u32[]{:S(2)}) copy-start(bf16[512,512]{1,0:T(8,128)(2,1)} %param.15) | copy-start | bytes 1572868
  33.4 17.0 %collective-permute-start = (bf16[2,2,512]{2,1,0:T(2,128)(2,1)S(1)}, bf16[2,2,512]{2,1,0:T(2,128)(2,1)S(1)}, u32[]{:S(2)}, u32[]{:S(2)}) collective-permute-start(bf16[2,2,512]{2,1,0:T(2,128)(2,1)S(1)} %pad_maximum_fusion.1), channel_id=1, source_target_pairs={{0,4},{4,8},{8,12},{12,16},{16,20},{20,24},{24,28},{1,5},{5,9},{9,... | collective-permute-start | bytes 12296 | tf_op jit(solution)/shard_map/ppermute | solution.py:14
  50.7 2.8 %copy-start.6 = (bf16[2048,256]{1,0:T(8,128)(2,1)S(1)}, bf16[2048,256]{1,0:T(8,128)(2,1)}, u32[]{:S(2)}) copy-start(bf16[2048,256]{1,0:T(8,128)(2,1)} %param.25) | copy-start | bytes 3145732
  145.9 4.0 %copy-start.2 = (bf16[1,1024,2048]{2,1,0:T(8,128)(2,1)S(1)}, bf16[1,1024,2048]{2,1,0:T(8,128)(2,1)}, u32[]{:S(2)}) copy-start(bf16[1,1024,2048]{2,1,0:T(8,128)(2,1)} %all-gather.11.cloned.1.call-done) | copy-start | bytes 12582916
  153.2 54.3 %all-to-all-start.1 = ((bf16[8,64,2048]{2,1,0:T(8,128)(2,1)}), bf16[8,64,2048]{2,1,0:T(8,128)(2,1)}, u32[]{:S(2)}, u32[]{:S(2)}) async-start(bf16[8,64,2048]{2,1,0:T(8,128)(2,1)} %bitcast.57), calls=%async_computation.2 | async-start | bytes 4194304 | tf_op jit(solution)/shard_map/all_to_all | solution.py:139
Sparse Core Ops, SparseCore 0:
  11.5 25.2 all-gather.4
  38.3 34.9 all-gather.6
  74.9 34.9 all-gather.8
  111.4 34.4 all-gather.10
  148.2 44.5 reduce-scatter.1
where the time goes:
time: 230 us; the launch traced here: 229 us
  waiting for transfers between devices  128 us (56%)
  matrix products  32.2 us (14%)
  other arithmetic  20.4 us (9%)
  starting transfers between devices  17.3 us (8%)
  local copies, waits for them, and re-layouts  17.2 us (7%)
  between operations  14 us (6%)
    all_to_all x1, waiting for transfers between devices, per_device(): lax.all_to_all(routed_back, 'ep', split_axis=0, concat_axis=0, tiled=True)  47.9 us
    all_gather x1, waiting for transfers between devices, per_device(): lax.all_gather(down_proj, 'tp', axis=1, tiled=True)  30 us
    all_gather x1, waiting for transfers between devices, per_device(): lax.all_gather(up_proj, 'tp', axis=2, tiled=True)  21.2 us
    all_to_all x1, waiting for transfers between devices, send_own(): lax.all_to_all(outgoing, 'ep', split_axis=0, concat_axis=0, tiled=True)  14.2 us
    ppermute x1, waiting for transfers between devices, shifted(): return lax.ppermute(block, axis, route)  12.8 us
    dot_general x2, matrix products, swiglu(): gate_term = jnp.dot(inputs, gate_w, preferred_element_type=jnp.float32)  10.3 us
    all_to_all x1, starting transfers between devices, send_own(): lax.all_to_all(outgoing, 'ep', split_axis=0, concat_axis=0, tiled=True)  7.44 us
    dot_general x4, matrix products, per_device(): jnp.dot(hidden[:, piece_idx * unit_block:(piece_idx + 1) * unit_block], d...  7.31 us
  transfers between devices with their start and end apart: 8, of which 5 were waited for; matrix products, arithmetic and copies ran while one was open for 27% of the time, Pallas kernels for 0%

commit v1 on v0

v1 whole, which is shorter than its diff:
```python
import functools

import jax
import jax.numpy as jnp
from jax import lax
from jax.experimental import pallas as pl
from jax.experimental.pallas import tpu as pltpu
from jax.sharding import PartitionSpec as P

epsilon = 1e-06
MESH = pl.DeviceIdType.MESH
f32 = jnp.float32
bf16 = jnp.bfloat16
CHUNKS = 4


def dot(a, b):
    return jnp.dot(a, b, preferred_element_type=f32)


def kernel(
    dims,
    outer, inner, values, taps, out_w, tokens, gain, gate_p, up_p, down_p,
    sh_gate, sh_up, sh_down, routes, weights,
    mix_o, exp_o,
    l_outer, l_inner, l_values, halo, prod, l_out_w, l_sg, l_su, l_sd,
    gf, uf, df, nf, og, ld, hid, rt, rv,
    parts, pairs, sums, arrived,
    loc_sem, halo_send, halo_recv, x_send, p_send, t_recv,
    d_send, d_recv, b_send, b_recv, r_send, r_recv, rx_send, rx_recv,
):
    ep, tp, cap = dims
    half = tp // 2
    e, t = lax.axis_index("ep"), lax.axis_index("tp")
    a, b = t // 2, lax.rem(t, 2)
    pair = (e, 2 * a + 1 - b)
    group, ch = l_inner.shape
    rows, width = tokens.shape
    slots = ep * cap
    cols = width // CHUNKS
    n_taps = taps.shape[0]

    def far(d):
        return 2 * lax.rem(a + d, half) + b

    def near(d):
        return 2 * lax.rem(a + half - d, half) + b

    def remote(src, dst, s, r, dev):
        return pltpu.make_async_remote_copy(
            src_ref=src, dst_ref=dst, send_sem=s, recv_sem=r, device_id=dev, device_id_type=MESH
        )

    barrier = pltpu.get_barrier_semaphore()

    def greet(d, _):
        pl.semaphore_signal(barrier, inc=1, device_id=(lax.rem(e + d, ep), t), device_id_type=MESH)
        return 0

    lax.fori_loop(1, ep, greet, 0)
    pl.semaphore_signal(barrier, inc=1, device_id=pair, device_id_type=MESH)
    for d in range(1, half):
        pl.semaphore_signal(barrier, inc=1, device_id=(e, far(d)), device_id_type=MESH)

    local = [
        pltpu.make_async_copy(s, d, loc_sem.at[i])
        for i, (s, d) in enumerate(
            (
                (inner, l_inner), (values, l_values), (outer, l_outer), (out_w, l_out_w),
                (sh_gate, l_sg), (sh_up, l_su), (sh_down, l_sd),
                (gate_p.at[0], gf.at[t]), (up_p.at[0], uf.at[t]), (down_p.at[0], df.at[t]),
            )
        )
    ]
    for c in local:
        c.start()

    def norm_rows(i, _):
        at = pl.ds(pl.multiple_of(i * 16, 16), 16)
        v = tokens[at, :].astype(f32)
        square = jnp.mean(v * v, axis=-1, keepdims=True)
        nf[t, at, :] = (v * lax.rsqrt(square + epsilon) * gain[...].astype(f32)).astype(bf16)
        return 0

    lax.fori_loop(0, rows // 16, norm_rows, 0)
    mine = pl.ds(pl.multiple_of(t * rows, rows), rows)
    own_routes, own_w = routes[mine, :], weights[mine, :]
    slot = lax.broadcasted_iota(jnp.int32, (rows, slots), 1)
    expert = slot // cap
    place = (slot - expert * cap).astype(f32)
    hit = jnp.zeros((rows, slots), f32)
    scale = jnp.zeros((rows, slots), f32)
    for k in range(own_routes.shape[1]):
        same = own_routes[:, k : k + 1] == expert
        hit = jnp.where(same, 1.0, hit)
        scale = jnp.where(same, own_w[:, k : k + 1], scale)
    lower = lax.broadcasted_iota(jnp.int32, (rows, rows), 0) > lax.broadcasted_iota(
        jnp.int32, (rows, rows), 1
    )
    earlier = dot(jnp.where(lower, 1.0, 0.0).astype(bf16), hit.astype(bf16))
    chosen = jnp.where(earlier == place, hit, 0.0)
    w_all = chosen * scale
    w_hi = w_all.astype(bf16)
    w_lo = (w_all - w_hi.astype(f32)).astype(bf16)
    sender = jnp.transpose(chosen).astype(bf16)

    pl.semaphore_wait(barrier, ep - 1 + 1 + half - 1)

    kinds = CHUNKS + 3
    n_kind = kinds - 1

    def land(k, s):
        if k == 0:
            return gf.at[s]
        if k == 1:
            return uf.at[s]
        if k == n_kind:
            return nf.at[s]
        return df.at[s, :, pl.ds((k - 2) * cols, cols)]

    def origin(k):
        if k == 0:
            return gate_p.at[0]
        if k == 1:
            return up_p.at[0]
        if k == n_kind:
            return nf.at[t]
        return down_p.at[0, :, pl.ds((k - 2) * cols, cols)]

    def x_copy(k, d):
        return remote(origin(k), land(k, t), x_send.at[k, d], t_recv.at[k, d], (e, far(d)))

    def pair_copy(k):
        return remote(origin(k), land(k, t), p_send.at[k, 0], t_recv.at[k, 0], pair)

    def forward_copy(k, d):
        s = near(d)
        return remote(land(k, s), land(k, s), p_send.at[k, d], t_recv.at[k, half - 1 + d], pair)

    def start_x(k):
        for d in range(1, half):
            x_copy(k, d).start()

    def forward(k):
        for d in range(1, half):
            x_copy(k, d).wait_recv()
            forward_copy(k, d).start()

    def wait_forwarded(k):
        for d in range(1, half):
            forward_copy(k, d).wait_recv()

    start_x(0)
    start_x(1)
    edge = pl.ds(group - 16, 16)
    halos = [
        remote(src.at[edge, :], halo.at[i], halo_send.at[i], halo_recv.at[i], (lax.rem(e + 1, ep), t))
        for i, src in enumerate((inner, values))
    ]
    for c in halos:
        c.start()

    def block(i):
        return pl.ds(pl.multiple_of(i * cap, cap), cap)

    def dispatch_copy(d):
        to = lax.rem(e + d, ep)
        return remote(og.at[block(to), :], ld.at[block(e), :], d_send.at[d], d_recv.at[d], (to, t))

    for c in range(CHUNKS):
        at = pl.ds(c * cols, cols)
        og[:, at] = dot(sender, nf[t, :, at]).astype(bf16)

    def start_dispatch(d, _):
        dispatch_copy(d).start()
        return 0

    lax.fori_loop(1, ep, start_dispatch, 0)
    ld[block(e), :] = og[block(e), :]
    for k in range(kinds):
        pair_copy(k).start()
    for k in range(2, kinds):
        start_x(k)

    def pair_sum(j, i):
        return remote(
            parts.at[j, 2 * i + 1 - b], pairs.at[j, i], r_send.at[j, i], r_recv.at[j, i], pair
        )

    def far_sum(j, d):
        return remote(
            sums.at[j, d - 1], arrived.at[j, d - 1], rx_send.at[j, d], rx_recv.at[j, d], (e, far(d))
        )

    def start_far(j):
        for d in range(1, half):
            i = lax.rem(a + d, half)
            pair_sum(j, i).wait_recv()
            for c in range(CHUNKS):
                at = pl.ds(c * cols, cols)
                total = parts[j, 2 * i + b, :, at].astype(f32) + pairs[j, i, :, at].astype(f32)
                sums[j, d - 1, :, at] = total.astype(bf16)
            far_sum(j, d).start()

    def finish_sum(j):
        pair_sum(j, a).wait_recv()
        for d in range(1, half):
            far_sum(j, d).wait_recv()

    def summed(j, at):
        total = parts[j, t, :, at].astype(f32) + pairs[j, a, :, at].astype(f32)
        for d in range(1, half):
            total = total + arrived[j, d - 1, :, at].astype(f32)
        return total

    for c in local[:4]:
        c.wait()
    for c in halos:
        c.wait_recv()
    before = halo[0].astype(f32) * halo[1].astype(f32)
    prod[0:16, :] = jnp.where(e > 0, before, 0.0)
    prod[16:, :] = l_inner[...].astype(f32) * l_values[...].astype(f32)
    tap = taps[...].astype(f32)
    for s in range(tp):
        lo = s * rows
        conv = jnp.zeros((rows, ch), f32)
        for j in range(n_taps):
            first = 16 + lo - (n_taps - 1) + j
            conv = conv + tap[j : j + 1, :] * prod[first : first + rows, :]
        gated = (l_outer[lo : lo + rows, :].astype(f32) * conv).astype(bf16)
        for c in range(CHUNKS):
            at = pl.ds(c * cols, cols)
            parts[0, s, :, at] = dot(gated, l_out_w[:, at]).astype(bf16)
    for i in range(half):
        pair_sum(0, i).start()

    for c in local[4:]:
        c.wait()

    def shared(s):
        x = nf[s]
        g = dot(x, l_sg[...])
        u = dot(x, l_su[...])
        h = (g / (1.0 + jnp.exp(-g)) * u).astype(bf16)
        for c in range(CHUNKS):
            at = pl.ds(c * cols, cols)
            parts[1, s, :, at] = dot(h, l_sd[:, at]).astype(bf16)

    shared(t)
    start_far(0)
    pair_copy(n_kind).wait_recv()
    shared(2 * a + 1 - b)
    pair_sum(1, a).start()

    def wait_dispatch(d, _):
        dispatch_copy(d).wait_recv()
        return 0

    lax.fori_loop(1, ep, wait_dispatch, 0)

    def hidden(s):
        g = dot(ld[...], gf[s])
        u = dot(ld[...], uf[s])
        hid[s] = (g / (1.0 + jnp.exp(-g)) * u).astype(bf16)

    hidden(t)
    pair_copy(0).wait_recv()
    pair_copy(1).wait_recv()
    hidden(2 * a + 1 - b)
    forward(0)
    forward(1)
    for d in range(1, half):
        hidden(near(d))
    wait_forwarded(0)
    wait_forwarded(1)
    for d in range(1, half):
        hidden(near(d) + 1 - 2 * b)

    def back_copy(c, d):
        to = lax.rem(e + d, ep)
        at = pl.ds(c * cols, cols)
        return remote(
            rt.at[block(to), at], rv.at[block(e), at], b_send.at[c, d], b_recv.at[c, d], (to, t)
        )

    for c in range(CHUNKS):
        k = 2 + c
        at = pl.ds(c * cols, cols)
        pair_copy(k).wait_recv()
        forward(k)
        wait_forwarded(k)
        total = dot(hid[0], df[0, :, at])
        for s in range(1, tp):
            total = total + dot(hid[s], df[s, :, at])
        rt[:, at] = total.astype(bf16)

        def start_back(d, _):
            back_copy(c, d).start()
            return 0

        lax.fori_loop(1, ep, start_back, 0)
        rv[block(e), at] = rt[block(e), at]

    forward(n_kind)
    for d in range(1, half):
        shared(near(d))
    wait_forwarded(n_kind)
    for d in range(1, half):
        shared(near(d) + 1 - 2 * b)
        pair_sum(1, lax.rem(a + half - d, half)).start()
    start_far(1)

    finish_sum(0)
    for c in range(CHUNKS):
        at = pl.ds(c * cols, cols)
        mix_o[:, at] = summed(0, at).astype(bf16)
    finish_sum(1)
    for c in range(CHUNKS):
        at = pl.ds(c * cols, cols)

        def wait_back(d, _):
            back_copy(c, d).wait_recv()
            return 0

        lax.fori_loop(1, ep, wait_back, 0)
        routed = dot(w_hi, rv[:, at]) + dot(w_lo, rv[:, at])
        exp_o[:, at] = (summed(1, at) + routed).astype(bf16)

    def sent(d, _):
        dispatch_copy(d).wait_send()
        for c in range(CHUNKS):
            back_copy(c, d).wait_send()
        return 0

    lax.fori_loop(1, ep, sent, 0)
    for c in halos:
        c.wait_send()
    for k in range(kinds):
        pair_copy(k).wait_send()
        for d in range(1, half):
            x_copy(k, d).wait_send()
            forward_copy(k, d).wait_send()
    for j in range(2):
        for i in range(half):
            pair_sum(j, i).wait_send()
        for d in range(1, half):
            far_sum(j, d).wait_send()


def per_device(
    outer_gate, inner_gate, conv_values, conv_taps, out_weight, moe_input, norm_gain,
    gate_proj, up_proj, down_proj, shared_gate, shared_up, shared_down, routes, route_weight,
):
    tp = lax.axis_size("tp")
    ep = lax.axis_size("ep")
    half = tp // 2
    group, ch = inner_gate.shape
    rows, width = moe_input.shape
    units = gate_proj.shape[2]
    sh_units = shared_gate.shape[1]
    cap = 2 * rows * routes.shape[1] // ep
    cap = -(-cap // 16) * 16
    slots = ep * cap
    kinds = CHUNKS + 3
    any_spec = pl.BlockSpec(memory_space=pl.ANY)
    vmem = pl.BlockSpec(memory_space=pltpu.VMEM)
    dma = pltpu.SemaphoreType.DMA

    def buf(*shape):
        return pltpu.VMEM(shape, bf16)

    scratch = [
        buf(group, ch), buf(group, ch), buf(group, ch), buf(2, 16, ch),
        pltpu.VMEM((group + 16, ch), f32), buf(ch, width),
        buf(width, sh_units), buf(width, sh_units), buf(sh_units, width),
        buf(tp, width, units), buf(tp, width, units), buf(tp, units, width),
        buf(tp, rows, width), buf(slots, width), buf(slots, width),
        buf(tp, slots, units), buf(slots, width), buf(slots, width),
        buf(2, tp, rows, width), buf(2, half, rows, width),
        buf(2, half - 1, rows, width), buf(2, half - 1, rows, width),
        dma((10,)), dma((2,)), dma((2,)), dma((kinds, half)), dma((kinds, half)),
        dma((kinds, tp)), dma((ep,)), dma((ep,)), dma((CHUNKS, ep)), dma((CHUNKS, ep)),
        dma((2, half)), dma((2, half)), dma((2, half)), dma((2, half)),
    ]
    out = jax.ShapeDtypeStruct((rows, width), bf16)
    return pl.pallas_call(
        functools.partial(kernel, (ep, tp, cap)),
        out_shape=(out, out),
        in_specs=[
            any_spec, any_spec, any_spec, vmem, any_spec, vmem, vmem,
            any_spec, any_spec, any_spec, any_spec, any_spec, any_spec, vmem, vmem,
        ],
        out_specs=(vmem, vmem),
        scratch_shapes=scratch,
        compiler_params=pltpu.CompilerParams(
            collective_id=0, has_side_effects=True, vmem_limit_bytes=67043328
        ),
    )(
        outer_gate, inner_gate, conv_values, conv_taps, out_weight, moe_input,
        norm_gain.reshape(1, width), gate_proj, up_proj, down_proj,
        shared_gate, shared_up, shared_down, routes, route_weight,
    )


def solution(mesh):
    return jax.shard_map(
        per_device,
        mesh=mesh,
        in_specs=(
            P("ep", "tp"), P("ep", "tp"), P("ep", "tp"), P(None, "tp"), P("tp", None),
            P(("ep", "tp"), None), P(),
            P("ep", None, "tp"), P("ep", None, "tp"), P("ep", "tp", None),
            P(None, "tp"), P(None, "tp"), P("tp", None), P("ep", None), P("ep", None),
        ),
        out_specs=(P(("ep", "tp"), None), P(("ep", "tp"), None)),
        check_vma=False,
    )
```

time: 230 us -> 124 us (0.54)
  waiting for transfers between devices: 128 us -> 0 us
  Pallas kernels: 0 us -> 114 us
  matrix products: 32.2 us -> 0 us
  other arithmetic: 20.4 us -> 0 us
  starting transfers between devices: 17.3 us -> 0 us
  between operations: 14 us -> 0.64 us
  local copies, waits for them, and re-layouts: 17.2 us -> 8.13 us
    pallas_call x0 -> x1, Pallas kernels: none -> 114 us  [per_device(): pl.pallas_call(functools.partial(kernel, (ep, tp, cap)), out_shape=(out,...]
    all_to_all x2 -> x0, waiting for transfers between devices: 62.2 us -> none  [the longest x1 47.9 us: per_device(): lax.all_to_all(routed_back, 'ep', split_axis=0, concat_axis=0, tiled=True)]
    all_gather x4 -> x0, waiting for transfers between devices: 51.2 us -> none  [the longest x1 30 us: per_device(): lax.all_gather(down_proj, 'tp', axis=1, tiled=True)]
    dot_general x9 -> x0, matrix products: 32.2 us -> none  [the longest x2 10.3 us: swiglu(): gate_term = jnp.dot(inputs, gate_w, preferred_element_type=jnp.float32)]
    all_to_all x2 -> x0, starting transfers between devices: 13 us -> none  [the longest x1 7.44 us: send_own(): lax.all_to_all(outgoing, 'ep', split_axis=0, concat_axis=0, tiled=True)]
    ppermute x1 -> x0, waiting for transfers between devices: 12.8 us -> none  [shifted(): return lax.ppermute(block, axis, route)]
    gather x2 -> x0, local copies, waits for them, and re-layouts: 7.54 us -> none  [the longest x1 4.22 us: per_device(): returned[own_targets].reshape(own_rows, top_count, model_width)]
    unnamed x16 -> x4, local copies, waits for them, and re-layouts: 0.04 us -> 6.84 us
  transfers between devices with their start and end apart: 8 -> 0, of which waited for: 5 -> 0; matrix products, arithmetic and copies ran while one was open for 27% -> 0% of each run, Pallas kernels for 0% -> 0%
where the time goes in v1:
time: 124 us; the launch traced here: 123 us
  Pallas kernels  114 us (92%)
  local copies, waits for them, and re-layouts  8.13 us (7%)
    pallas_call x1, Pallas kernels, per_device(): pl.pallas_call(functools.partial(kernel, (ep, tp, cap)), out_shape=(out,...  114 us
    unnamed x4, local copies, waits for them, and re-layouts  6.84 us

profile of v1, /device:TPU:0, one launch (start us, length us, event | category | flops | bytes accessed | tf_op | source)
XLA Modules:
  0.0 123.2 jit_solution(10542838732201663205)
XLA Ops:
  0.6 1.3 %reshape.7.gain = bf16[1,2048]{1,0:T(2,128)(2,1)} reshape(bf16[2048]{0:T(1024)(128)(2,1)} %param.21) | data formatting | bytes 8192 | tf_op jit(solution)/shard_map/reshape | solution.py:400
  1.9 1.5 %copy.17.routes = s32[512,2]{1,0:T(8,128)} copy(s32[512,2]{0,1:T(2,128)} %param.28) | data formatting | bytes 8192 | tf_op args[13]
  3.5 1.5 %copy.18.weights = f32[512,2]{1,0:T(8,128)} copy(f32[512,2]{0,1:T(2,128)} %param.29) | data formatting | bytes 8192 | tf_op args[14]
  5.0 114.4 %shard_map.158 = (bf16[128,2048]{1,0:T(8,128)(2,1)}, bf16[128,2048]{1,0:T(8,128)(2,1)}) custom-call(bf16[512,512]{1,0:T(8,128)(2,1)} %outer.1, bf16[512,512]{1,0:T(8,128)(2,1)} %inner.1, bf16[512,512]{1,0:T(8,128)(2,1)} %values.1, bf16[3,512]{1,0:T(4,128)(2,1)} %taps.1, bf16[512,2048]{1,0:T(8,128)(2,1)} %out_w.1, bf16[128,2048]{1,0:T(8,128)(2,1)} %tokens.1, ...), custom_call_target="tpu_custom_call" | custom-call | tf_op jit(solution)/shard_map/pallas_call | solution.py:386
  119.5 1.9 %copy.21 = bf16[128,2048]{1,0:T(8,128)(2,1)} copy(bf16[128,2048]{1,0:T(8,128)(2,1)} %get-tuple-element.4) | data formatting | bytes 1048576
  121.3 1.9 %copy.22 = bf16[128,2048]{1,0:T(8,128)(2,1)} copy(bf16[128,2048]{1,0:T(8,128)(2,1)} %get-tuple-element.5) | data formatting | bytes 1048576

commit v2 on v1

--- a/solution.py
+++ b/solution.py
@@ -25,7 +25,7 @@
     mix_o, exp_o,
     l_outer, l_inner, l_values, halo, prod, l_out_w, l_sg, l_su, l_sd,
     gf, uf, df, nf, og, ld, hid, rt, rv,
-    parts, pairs, sums, arrived,
+    acc, parts, pairs, sums, arrived,
     loc_sem, halo_send, halo_recv, x_send, p_send, t_recv,
     d_send, d_recv, b_send, b_recv, r_send, r_recv, rx_send, rx_recv,
 ):
@@ -75,35 +75,6 @@
     for c in local:
         c.start()
 
-    def norm_rows(i, _):
-        at = pl.ds(pl.multiple_of(i * 16, 16), 16)
-        v = tokens[at, :].astype(f32)
-        square = jnp.mean(v * v, axis=-1, keepdims=True)
-        nf[t, at, :] = (v * lax.rsqrt(square + epsilon) * gain[...].astype(f32)).astype(bf16)
-        return 0
-
-    lax.fori_loop(0, rows // 16, norm_rows, 0)
-    mine = pl.ds(pl.multiple_of(t * rows, rows), rows)
-    own_routes, own_w = routes[mine, :], weights[mine, :]
-    slot = lax.broadcasted_iota(jnp.int32, (rows, slots), 1)
-    expert = slot // cap
-    place = (slot - expert * cap).astype(f32)
-    hit = jnp.zeros((rows, slots), f32)
-    scale = jnp.zeros((rows, slots), f32)
-    for k in range(own_routes.shape[1]):
-        same = own_routes[:, k : k + 1] == expert
-        hit = jnp.where(same, 1.0, hit)
-        scale = jnp.where(same, own_w[:, k : k + 1], scale)
-    lower = lax.broadcasted_iota(jnp.int32, (rows, rows), 0) > lax.broadcasted_iota(
-        jnp.int32, (rows, rows), 1
-    )
-    earlier = dot(jnp.where(lower, 1.0, 0.0).astype(bf16), hit.astype(bf16))
-    chosen = jnp.where(earlier == place, hit, 0.0)
-    w_all = chosen * scale
-    w_hi = w_all.astype(bf16)
-    w_lo = (w_all - w_hi.astype(f32)).astype(bf16)
-    sender = jnp.transpose(chosen).astype(bf16)
-
     pl.semaphore_wait(barrier, ep - 1 + 1 + half - 1)
 
     kinds = CHUNKS + 3
@@ -150,8 +121,57 @@
         for d in range(1, half):
             forward_copy(k, d).wait_recv()
 
-    start_x(0)
-    start_x(1)
+    for k in range(4):
+        start_x(k)
+    mine = pl.ds(pl.multiple_of(t * rows, rows), rows)
+    own_routes, own_w = routes[:, mine], weights[:, mine]
+    slot = lax.broadcasted_iota(jnp.int32, (slots, rows), 0)
+    expert = slot // cap
+    place = (slot - expert * cap).astype(f32)
+    hit = jnp.zeros((slots, rows), f32)
+    for k in range(own_routes.shape[0]):
+        hit = jnp.where(own_routes[k : k + 1, :] == expert, 1.0, hit)
+    upper = lax.broadcasted_iota(jnp.int32, (rows, rows), 0) < lax.broadcasted_iota(
+        jnp.int32, (rows, rows), 1
+    )
+    earlier = dot(hit.astype(bf16), jnp.where(upper, 1.0, 0.0).astype(bf16))
+    chosen = jnp.where(earlier == place, hit, 0.0)
+    sender = chosen.astype(bf16)
+
+    def norm_rows(i, _):
+        at = pl.ds(pl.multiple_of(i * 16, 16), 16)
+        v = tokens[at, :].astype(f32)
+        square = jnp.mean(v * v, axis=-1, keepdims=True)
+        nf[t, at, :] = (v * lax.rsqrt(square + epsilon) * gain[...].astype(f32)).astype(bf16)
+        return 0
+
+    lax.fori_loop(0, rows // 16, norm_rows, 0)
+
+    def block(i):
+        return pl.ds(pl.multiple_of(i * cap, cap), cap)
+
+    def dispatch_copy(c, d):
+        to = lax.rem(e + d, ep)
+        at = pl.ds(c * cols, cols)
+        return remote(
+            og.at[block(to), at], ld.at[block(e), at], d_send.at[c, d], d_recv.at[c, d], (to, t)
+        )
+
+    for c in range(CHUNKS):
+        at = pl.ds(c * cols, cols)
+        og[:, at] = dot(sender, nf[t, :, at]).astype(bf16)
+
+        def start_dispatch(d, _):
+            dispatch_copy(c, d).start()
+            return 0
+
+        lax.fori_loop(1, ep, start_dispatch, 0)
+        ld[block(e), at] = og[block(e), at]
+    start_x(n_kind)
+    for k in range(kinds):
+        pair_copy(k).start()
+    for k in range(4, n_kind):
+        start_x(k)
     edge = pl.ds(group - 16, 16)
     halos = [
         remote(src.at[edge, :], halo.at[i], halo_send.at[i], halo_recv.at[i], (lax.rem(e + 1, ep), t))
@@ -160,27 +180,6 @@
     for c in halos:
         c.start()
 
-    def block(i):
-        return pl.ds(pl.multiple_of(i * cap, cap), cap)
-
-    def dispatch_copy(d):
-        to = lax.rem(e + d, ep)
-        return remote(og.at[block(to), :], ld.at[block(e), :], d_send.at[d], d_recv.at[d], (to, t))
-
-    for c in range(CHUNKS):
-        at = pl.ds(c * cols, cols)
-        og[:, at] = dot(sender, nf[t, :, at]).astype(bf16)
-
-    def start_dispatch(d, _):
-        dispatch_copy(d).start()
-        return 0
-
-    lax.fori_loop(1, ep, start_dispatch, 0)
-    ld[block(e), :] = og[block(e), :]
-    for k in range(kinds):
-        pair_copy(k).start()
-    for k in range(2, kinds):
-        start_x(k)
 
     def pair_sum(j, i):
         return remote(
@@ -247,34 +246,43 @@
             parts[1, s, :, at] = dot(h, l_sd[:, at]).astype(bf16)
 
     shared(t)
-    start_far(0)
     pair_copy(n_kind).wait_recv()
     shared(2 * a + 1 - b)
     pair_sum(1, a).start()
 
-    def wait_dispatch(d, _):
-        dispatch_copy(d).wait_recv()
-        return 0
-
-    lax.fori_loop(1, ep, wait_dispatch, 0)
-
-    def hidden(s):
-        g = dot(ld[...], gf[s])
-        u = dot(ld[...], uf[s])
+    def act(s, g, u):
         hid[s] = (g / (1.0 + jnp.exp(-g)) * u).astype(bf16)
 
-    hidden(t)
     pair_copy(0).wait_recv()
     pair_copy(1).wait_recv()
-    hidden(2 * a + 1 - b)
-    forward(0)
+    close = (t, 2 * a + 1 - b)
+    for c in range(CHUNKS):
+        at = pl.ds(c * cols, cols)
+
+        def wait_dispatch(d, _):
+            dispatch_copy(c, d).wait_recv()
+            return 0
+
+        lax.fori_loop(1, ep, wait_dispatch, 0)
+        for i, s in enumerate(close):
+            g, u = dot(ld[:, at], gf[s, at, :]), dot(ld[:, at], uf[s, at, :])
+            if c:
+                g, u = g + acc[i, 0], u + acc[i, 1]
+            if c < CHUNKS - 1:
+                acc[i, 0] = g
+                acc[i, 1] = u
+            else:
+                act(s, g, u)
+        if c == 1:
+            forward(0)
+    wait_forwarded(0)
+    rest = [near(d) for d in range(1, half)] + [near(d) + 1 - 2 * b for d in range(1, half)]
+    gates = [dot(ld[...], gf[s]) for s in rest]
     forward(1)
-    for d in range(1, half):
-        hidden(near(d))
-    wait_forwarded(0)
-    wait_forwarded(1)
-    for d in range(1, half):
-        hidden(near(d) + 1 - 2 * b)
+    for n, s in enumerate(rest):
+        if n == half - 1:
+            wait_forwarded(1)
+        act(s, gates[n], dot(ld[...], uf[s]))
 
     def back_copy(c, d):
         to = lax.rem(e + d, ep)
@@ -300,20 +308,23 @@
 
         lax.fori_loop(1, ep, start_back, 0)
         rv[block(e), at] = rt[block(e), at]
-
-    forward(n_kind)
-    for d in range(1, half):
-        shared(near(d))
-    wait_forwarded(n_kind)
-    for d in range(1, half):
-        shared(near(d) + 1 - 2 * b)
-        pair_sum(1, lax.rem(a + half - d, half)).start()
-    start_far(1)
-
-    finish_sum(0)
-    for c in range(CHUNKS):
-        at = pl.ds(c * cols, cols)
-        mix_o[:, at] = summed(0, at).astype(bf16)
+        if c == 1:
+            forward(n_kind)
+            for d in range(1, half):
+                shared(near(d))
+            wait_forwarded(n_kind)
+            for d in range(1, half):
+                shared(near(d) + 1 - 2 * b)
+                pair_sum(1, lax.rem(a + half - d, half)).start()
+            start_far(1)
+            start_far(0)
+
+    scale = jnp.zeros((slots, rows), f32)
+    for k in range(own_routes.shape[0]):
+        scale = jnp.where(own_routes[k : k + 1, :] == expert, own_w[k : k + 1, :], scale)
+    w_all = jnp.transpose(chosen * scale)
+    w_hi = w_all.astype(bf16)
+    w_lo = (w_all - w_hi.astype(f32)).astype(bf16)
     finish_sum(1)
     for c in range(CHUNKS):
         at = pl.ds(c * cols, cols)
@@ -326,9 +337,13 @@
         routed = dot(w_hi, rv[:, at]) + dot(w_lo, rv[:, at])
         exp_o[:, at] = (summed(1, at) + routed).astype(bf16)
 
+    finish_sum(0)
+    for c in range(CHUNKS):
+        at = pl.ds(c * cols, cols)
+        mix_o[:, at] = summed(0, at).astype(bf16)
     def sent(d, _):
-        dispatch_copy(d).wait_send()
         for c in range(CHUNKS):
+            dispatch_copy(c, d).wait_send()
             back_copy(c, d).wait_send()
         return 0
 
@@ -376,10 +391,10 @@
         buf(tp, width, units), buf(tp, width, units), buf(tp, units, width),
         buf(tp, rows, width), buf(slots, width), buf(slots, width),
         buf(tp, slots, units), buf(slots, width), buf(slots, width),
-        buf(2, tp, rows, width), buf(2, half, rows, width),
+        pltpu.VMEM((2, 2, slots, units), f32), buf(2, tp, rows, width), buf(2, half, rows, width),
         buf(2, half - 1, rows, width), buf(2, half - 1, rows, width),
         dma((10,)), dma((2,)), dma((2,)), dma((kinds, half)), dma((kinds, half)),
-        dma((kinds, tp)), dma((ep,)), dma((ep,)), dma((CHUNKS, ep)), dma((CHUNKS, ep)),
+        dma((kinds, tp)), dma((CHUNKS, ep)), dma((CHUNKS, ep)), dma((CHUNKS, ep)), dma((CHUNKS, ep)),
         dma((2, half)), dma((2, half)), dma((2, half)), dma((2, half)),
     ]
     out = jax.ShapeDtypeStruct((rows, width), bf16)
@@ -398,7 +413,7 @@
     )(
         outer_gate, inner_gate, conv_values, conv_taps, out_weight, moe_input,
         norm_gain.reshape(1, width), gate_proj, up_proj, down_proj,
-        shared_gate, shared_up, shared_down, routes, route_weight,
+        shared_gate, shared_up, shared_down, routes.T, route_weight.T,
     )
 
 

time: 124 us -> 119 us (0.960)
  local copies, waits for them, and re-layouts: 8.13 us -> 5.05 us
    unnamed x4 -> x2, local copies, waits for them, and re-layouts: 6.84 us -> 3.76 us
where the time goes in v2:
time: 119 us
  Pallas kernels  114 us (96%)
  local copies, waits for them, and re-layouts  5.05 us (4%)
    pallas_call x1, Pallas kernels, per_device(): pl.pallas_call(functools.partial(kernel, (ep, tp, cap)), out_shape=(out,...  114 us
    unnamed x2, local copies, waits for them, and re-layouts  3.76 us

profile of v2, /device:TPU:0, one launch (start us, length us, event | category | flops | bytes accessed | tf_op | source)
XLA Modules:
  0.0 119.2 jit_solution(10561458440216949077)
XLA Ops:
  0.6 1.3 %reshape.7.gain = bf16[1,2048]{1,0:T(2,128)(2,1)} reshape(bf16[2048]{0:T(1024)(128)(2,1)} %param.21) | data formatting | bytes 8192 | tf_op jit(solution)/shard_map/reshape | solution.py:415
  1.9 113.5 %shard_map.158 = (bf16[128,2048]{1,0:T(8,128)(2,1)}, bf16[128,2048]{1,0:T(8,128)(2,1)}) custom-call(bf16[512,512]{1,0:T(8,128)(2,1)} %outer.1, bf16[512,512]{1,0:T(8,128)(2,1)} %inner.1, bf16[512,512]{1,0:T(8,128)(2,1)} %values.1, bf16[3,512]{1,0:T(4,128)(2,1)} %taps.1, bf16[512,2048]{1,0:T(8,128)(2,1)} %out_w.1, bf16[128,2048]{1,0:T(8,128)(2,1)} %tokens.1, ...), custom_call_target="tpu_custom_call" | custom-call | tf_op jit(solution)/shard_map/pallas_call | solution.py:401
  115.5 1.9 %copy.19 = bf16[128,2048]{1,0:T(8,128)(2,1)} copy(bf16[128,2048]{1,0:T(8,128)(2,1)} %get-tuple-element.4) | data formatting | bytes 1048576
  117.3 1.9 %copy.20 = bf16[128,2048]{1,0:T(8,128)(2,1)} copy(bf16[128,2048]{1,0:T(8,128)(2,1)} %get-tuple-element.5) | data formatting | bytes 1048576

commit v3 on v2

--- a/solution.py
+++ b/solution.py
@@ -138,11 +138,13 @@
     chosen = jnp.where(earlier == place, hit, 0.0)
     sender = chosen.astype(bf16)
 
+    scales = gain[...].astype(f32).reshape(1, width)
+
     def norm_rows(i, _):
         at = pl.ds(pl.multiple_of(i * 16, 16), 16)
         v = tokens[at, :].astype(f32)
         square = jnp.mean(v * v, axis=-1, keepdims=True)
-        nf[t, at, :] = (v * lax.rsqrt(square + epsilon) * gain[...].astype(f32)).astype(bf16)
+        nf[t, at, :] = (v * lax.rsqrt(square + epsilon) * scales).astype(bf16)
         return 0
 
     lax.fori_loop(0, rows // 16, norm_rows, 0)
@@ -397,7 +399,7 @@
         dma((kinds, tp)), dma((CHUNKS, ep)), dma((CHUNKS, ep)), dma((CHUNKS, ep)), dma((CHUNKS, ep)),
         dma((2, half)), dma((2, half)), dma((2, half)), dma((2, half)),
     ]
-    out = jax.ShapeDtypeStruct((rows, width), bf16)
+    out = pltpu.VMEM((rows, width), bf16)
     return pl.pallas_call(
         functools.partial(kernel, (ep, tp, cap)),
         out_shape=(out, out),
@@ -408,11 +410,11 @@
         out_specs=(vmem, vmem),
         scratch_shapes=scratch,
         compiler_params=pltpu.CompilerParams(
-            collective_id=0, has_side_effects=True, vmem_limit_bytes=67043328
+            collective_id=0, has_side_effects=True, vmem_limit_bytes=65536000
         ),
     )(
         outer_gate, inner_gate, conv_values, conv_taps, out_weight, moe_input,
-        norm_gain.reshape(1, width), gate_proj, up_proj, down_proj,
+        norm_gain, gate_proj, up_proj, down_proj,
         shared_gate, shared_up, shared_down, routes.T, route_weight.T,
     )
 

time: 119 us -> 115 us (0.966)
  local copies, waits for them, and re-layouts: 5.05 us -> 1.59 us
    unnamed x2, local copies, waits for them, and re-layouts: 3.76 us -> 1.59 us
    reshape x1 -> x0, local copies, waits for them, and re-layouts: 1.29 us -> none  [per_device(): norm_gain.reshape(1, width)]
where the time goes in v3:
time: 115 us
  Pallas kernels  113 us (98%)
  local copies, waits for them, and re-layouts  1.59 us (1%)
    pallas_call x1, Pallas kernels, per_device(): pl.pallas_call(functools.partial(kernel, (ep, tp, cap)), out_shape=(out,...  113 us

profile of v3, /device:TPU:0, one launch (start us, length us, event | category | flops | bytes accessed | tf_op | source)
XLA Modules:
  0.0 114.8 jit_solution(2362242550939017188)
XLA Ops:
  0.6 112.5 %shard_map.158 = (bf16[128,2048]{1,0:T(8,128)(2,1)S(1)}, bf16[128,2048]{1,0:T(8,128)(2,1)S(1)}) custom-call(bf16[512,512]{1,0:T(8,128)(2,1)} %outer.1, bf16[512,512]{1,0:T(8,128)(2,1)} %inner.1, bf16[512,512]{1,0:T(8,128)(2,1)} %values.1, bf16[3,512]{1,0:T(4,128)(2,1)} %taps.1, bf16[512,2048]{1,0:T(8,128)(2,1)} %out_w.1, bf16[128,2048]{1,0:T(8,128)(2,1)} %tokens.1, ...), custom_call_target="tpu_custom_call" | custom-call | tf_op jit(solution)/shard_map/pallas_call | solution.py:403
  113.2 0.8 copy.19
  114.0 0.8 copy.20
